TPU v7x, 256 devices: a 4x2x16 block of a 4x16x16 slice. The times are simulated.
256 devices in a mesh: grp: 2 (over y), sp: 32 (over z, core), tp: 4 (over x).
Axes of the slice: x: 4, y: 2, z: 16, core: 2. Of those that a mesh axis runs over, the one named last changes fastest.
The devices are a block of a 4x16x16 slice.
Arguments:
- resid: bfloat16 [32768, 2048], P(('grp', 'sp', 'tp')), parts along dimension 0, may hold values from -6 to 6
- pool_input: bfloat16 [32768, 512], P(('grp', 'sp'), 'tp'), parts along dimension 0, may hold values from -6 to 6
- group_map: bfloat16 [4, 128, 128], P('tp'), may hold values from -0.5 to 0.5
- pool_scale: bfloat16 [512], P('tp'), may hold values from 0.099609375 to 1.8984375
- out_proj: bfloat16 [512, 2048], P('tp'), may hold values from -0.25 to 0.25
- norm_gain: bfloat16 [2048], replicated, may hold values from 0.099609375 to 1.8984375
- routes: int32 [32768, 2], P(('grp', 'sp', 'tp')), parts along dimension 0, may hold values from 0 to 31, all different within a row; in each aligned block of 128 rows (0 to 127, 128 to 255, ...) at most 10 rows name the same one
- route_weight: float32 [32768, 2], P(('grp', 'sp', 'tp')), parts along dimension 0, may hold values from 0.2 to 1
- expert_gate: bfloat16 [32, 2048, 3584], P('sp', None, 'tp'), may hold values from -0.125 to 0.125
- expert_up: bfloat16 [32, 2048, 3584], P('sp', None, 'tp'), may hold values from -0.125 to 0.125
- expert_down: bfloat16 [32, 3584, 2048], P('sp', 'tp'), may hold values from -0.09375 to 0.09375
Outputs:
- layer_out: bfloat16 [32768, 2048], P(('grp', 'sp', 'tp')), parts along dimension 0
There are 2 independent parts, one for each index of `grp`. A program takes and returns all parts, laid end to end along the dimension named above; an argument that names none is the same for every part. Nothing has to cross between parts.
Inputs may be any that keep to these rules, and one draw needn't show every extreme that they name: The 2 routes of a token differ. Among the tokens of one device (aligned blocks of 128 tokens), no expert is named more than 10 times, and in every draw some device names some expert exactly 10 times.
All inputs are finite; a program needn't handle non-finite values.
Results may differ from a plain program's by a relative error of at most 0.011.
Values may be sent and summed in bfloat16 or wider, within the bound.
A program may use at most 128 MiB of HBM per device.

v0:
```python
import jax
import jax.numpy as jnp
from jax import lax
from jax.sharding import PartitionSpec as P

GROUPS = 4


norm_eps = 1e-06


def from_behind(value, axis, steps):
    count = lax.axis_size(axis)
    leading, last = (max(0, -steps), min(count, count - steps))
    return lax.ppermute(value, axis, [(source, source + steps) for source in range(leading, last)])


def copy_for_each(value, axis):
    count = lax.axis_size(axis)
    return lax.all_to_all(
        jnp.broadcast_to(value[None], (count, *value.shape)), axis, 0, 0, tiled=True
    )


def in_order(tiles, dim):
    tiles = jnp.moveaxis(tiles, 0, dim)
    shape = tiles.shape
    return tiles.reshape(*shape[:dim], shape[dim] * shape[dim + 1], *shape[dim + 2 :])


def collect(value, axis, dim):
    tiles = copy_for_each(value, axis)
    return in_order(tiles, dim)


def grouped_exchange(value, axis, split_dim, concat_dim, work, item_dim, out_dim):
    items = jax.tree.leaves(value)[0].shape[item_dim]
    count = 2 if items % 2 == 0 else 1
    gathered = []
    for k in range(count):
        group = jax.tree.map(
            lambda a: lax.slice_in_dim(
                a, k * (items // count), (k + 1) * (items // count), axis=item_dim
            ),
            value,
        )
        gathered.append(
            work(
                lax.all_to_all(
                    group, axis, split_axis=split_dim, concat_axis=concat_dim, tiled=True
                )
            )
        )
    return jax.tree.map(lambda *parts: jnp.concatenate(parts, axis=out_dim), *gathered)


def split_up(value, dim, count):
    before, after = (value.shape[:dim], value.shape[dim + 1 :])
    return jnp.moveaxis(value.reshape(*before, count, -1, *after), dim, 0)


def sent_and_summed(value, axis, dim):
    count = lax.axis_size(axis)
    tiles = lax.all_to_all(split_up(value, dim, count), axis, 0, 0, tiled=True)
    return jnp.sum(tiles.astype(jnp.float32), axis=0)


def expert_block(arrived, gate_w, up_w, down_w):
    width = arrived.shape[-1]
    flat = arrived.reshape(-1, width)
    gate = jnp.dot(flat, gate_w, preferred_element_type=jnp.float32)
    up_value = jnp.dot(flat, up_w, preferred_element_type=jnp.float32)
    hidden = (jax.nn.silu(gate) * up_value).astype(jnp.bfloat16)
    partial_out = jnp.dot(hidden, down_w, preferred_element_type=jnp.float32).astype(jnp.bfloat16)
    return partial_out.reshape(arrived.shape)


def local(
    resid,
    pool_input,
    group_map,
    pool_scale,
    out_proj,
    norm_gain,
    routes,
    route_weight,
    expert_gate,
    expert_up,
    expert_down,
):
    seq_rows = pool_input.shape[0]
    local_groups = group_map.shape[0]
    group_dim = group_map.shape[1]
    reach = 2**GROUPS - 1
    rim_rows = from_behind(pool_input[seq_rows - reach :], "sp", 1)
    extended = jnp.concatenate([rim_rows, pool_input], axis=0).astype(jnp.float32)
    positions = lax.axis_index("sp") * seq_rows + jnp.arange(1, seq_rows + 1, dtype=jnp.int32)
    group = lax.axis_index("tp") * local_groups + 0
    window = jnp.left_shift(jnp.int32(2), group)
    window_sum = jnp.zeros((seq_rows, group_dim), jnp.float32)
    for back in range(reach + 1):
        window_sum = window_sum + jnp.where(
            back < window, extended[reach - back : reach - back + seq_rows], jnp.float32(0.0)
        )
    divisor = jnp.minimum(positions, window).astype(jnp.float32)
    pooled = (window_sum / divisor[:, None] - extended[reach:]).astype(jnp.bfloat16)
    product = jnp.dot(pooled, group_map[0], preferred_element_type=jnp.float32)
    scale = pool_scale.astype(jnp.float32)
    pieces = (product * scale).astype(jnp.bfloat16)
    own_rows = resid.shape[0]
    width = resid.shape[1]
    token_rows = lax.all_to_all(pieces, "tp", split_axis=0, concat_axis=1, tiled=True)
    mix = jnp.dot(token_rows, collect(out_proj, "tp", 0), preferred_element_type=jnp.float32)
    mixed = (resid.astype(jnp.float32) + mix).astype(jnp.bfloat16)
    residual = mixed.astype(jnp.float32)
    scaled = residual * lax.rsqrt(jnp.mean(residual * residual, axis=1, keepdims=True) + norm_eps)
    normed = (scaled * norm_gain.astype(jnp.float32)).astype(jnp.bfloat16)
    top_count = routes.shape[1]
    lanes = lax.axis_size("tp")
    seq_devices = lax.axis_size("sp")
    experts = seq_devices * expert_gate.shape[0]
    slots = max(2, 5 * own_rows * top_count // (4 * experts))
    flat_routes = routes.reshape(-1)
    onehot = (flat_routes[:, None] == jnp.arange(experts, dtype=jnp.int32)[None, :]).astype(
        jnp.int32
    )
    ranks = jnp.cumsum(onehot, axis=0) - onehot
    slot_of = jnp.sum(ranks * onehot, axis=1)
    target = flat_routes * slots + slot_of
    placing = (jnp.arange(experts * slots, dtype=jnp.int32)[:, None] == target[None, :]).astype(
        jnp.bfloat16
    )
    repeated = jnp.repeat(normed, top_count, axis=0)
    send_rows = jnp.dot(placing, repeated, preferred_element_type=jnp.float32).astype(jnp.bfloat16)
    gate_w = expert_gate[0]
    up_w = expert_up[0]
    down_w = expert_down[0]

    def compute(arrived):
        return expert_block(arrived, gate_w, up_w, down_w)

    def fanned_compute(arrived):
        everyone = lax.all_gather(arrived[:, None], "tp", axis=1, tiled=True)
        return compute(everyone.reshape(-1, everyone.shape[2], everyone.shape[3]))

    partials = grouped_exchange(
        send_rows.reshape(experts, slots, width), "sp", 0, 0, fanned_compute, 1, 1
    )
    quarter_terms = partials.astype(jnp.float32).reshape(seq_devices, lanes, slots, width)
    route_sums = sent_and_summed(quarter_terms.astype(jnp.bfloat16), "tp", 1)
    homeward = lax.all_to_all(
        route_sums.astype(jnp.bfloat16), "sp", split_axis=0, concat_axis=0, tiled=True
    ).astype(route_sums.dtype)
    summed = homeward.reshape(experts * slots, width)
    picked = jnp.take(summed, target, axis=0).reshape(own_rows, top_count, width)
    moe = jnp.sum(picked * route_weight[:, :, None], axis=1)
    return (residual + moe).astype(jnp.bfloat16)


def solution(mesh):
    return jax.shard_map(
        local,
        mesh=mesh,
        in_specs=(
            P(("grp", "sp", "tp"), None),
            P(("grp", "sp"), "tp"),
            P("tp", None, None),
            P("tp"),
            P("tp", None),
            P(),
            P(("grp", "sp", "tp"), None),
            P(("grp", "sp", "tp"), None),
            P("sp", None, "tp"),
            P("sp", None, "tp"),
            P("sp", "tp", None),
        ),
        out_specs=P(("grp", "sp", "tp"), None),
        check_vma=False,
    )
```

profile of v0, /device:TPU:33, one launch (start us, length us, event | category | flops | bytes accessed | tf_op | source)
XLA Modules:
  0.0 480.7 jit_solution(3502197953187652395)
XLA Ops:
  6.6 0.7 slice.64
  7.2 5.7 %collective-permute-start = (bf16[15,128]{1,0:T(8,128)(2,1)S(1)}, bf16[15,128]{1,0:T(8,128)(2,1)S(1)}, u32[]{:S(2)}, u32[]{:S(2)}) collective-permute-start(bf16[15,128]{1,0:T(8,128)(2,1)S(1)} %slice.64), channel_id=1, source_target_pairs={{0,4},{4,8},{8,12},{12,16},{16,20},{20,24},{24,28},{28,32},{32,36}... | collective-permute-start | bytes 11528 | tf_op jit(solution)/shard_map/ppermute | solution.py:15
  13.0 0.7 convert_element_type.72
  13.7 15.9 %collective-permute-done = bf16[15,128]{1,0:T(8,128)(2,1)S(1)} collective-permute-done((bf16[15,128]{1,0:T(8,128)(2,1)S(1)}, bf16[15,128]{1,0:T(8,128)(2,1)S(1)}, u32[]{:S(2)}, u32[]{:S(2)}) %collective-permute-start) | collective-permute-done | bytes 3872 | tf_op jit(solution)/shard_map/ppermute | solution.py:15
  29.6 0.9 maximum_convert_fusion
  30.5 0.0 copy-start.6
  30.6 0.7 fusion.25
  31.3 7.3 %all_to_all.41 = bf16[4,128,128]{2,1,0:T(8,128)(2,1)S(1)} all-to-all(bf16[4,128,128]{2,1,0:T(8,128)(2,1)S(1)} %bitcast.75), channel_id=1, replica_groups=mesh['grp'=2,'sp'=32,'tp'=4] {'tp'}, dimensions={0} | all-to-all | bytes 262144 | tf_op jit(solution)/shard_map/all_to_all | solution.py:112
  38.6 1.6 broadcast_in_dim.53
  40.2 3.8 all-to-all-start.1
  44.0 0.1 all-gather.5.cloned.1.call-start
  44.1 0.1 copy.40
  44.2 0.1 eq.39
  44.4 0.1 reshape.118
  44.6 0.6 reduce-window.6
  45.2 0.2 slice_reduce_fusion
  45.4 0.1 fusion.53
  45.5 23.6 %all-to-all-done.1 = bf16[4,128,2048]{2,1,0:T(8,128)(2,1)S(1)} async-done(((bf16[4,128,2048]{2,1,0:T(8,128)(2,1)}), bf16[4,128,2048]{2,1,0:T(8,128)(2,1)S(1)}, u32[]{:S(2)}, u32[]{:S(2)}) %all-to-all-start.1) | async-done | bytes 2097184 | tf_op jit(solution)/shard_map/all_to_all | solution.py:20
  69.1 0.0 copy-done.7
  69.1 0.6 multiply_reduce_fusion.1
  69.7 1.0 copy-done.2
  70.6 0.2 multiply_convert_fusion.2
  70.8 0.6 broadcast_in_dim.55
  71.4 0.4 reshape.120
  71.9 0.5 convolution_convert_fusion
  72.4 0.5 reshape.121
  72.9 0.5 fusion.59
  73.3 65.9 %all_to_all.42 = bf16[32,5,2048]{2,1,0:T(8,128)(2,1)S(1)} all-to-all(bf16[32,5,2048]{2,1,0:T(8,128)(2,1)S(1)} %get-tuple-element.5), channel_id=1, replica_groups=mesh['grp'=2,'sp'=32,'tp'=4] {'sp'}, dimensions={0} | all-to-all | bytes 1310720 | tf_op jit(solution)/shard_map/all_to_all | solution.py:49
  139.2 1.3 copy.45
  140.5 0.1 all-gather.5.cloned.1.call-update
  140.6 0.1 all-gather.7.cloned.1.call-start
  140.6 59.2 %all_to_all.43 = bf16[32,5,2048]{2,1,0:T(8,128)(2,1)S(1)} all-to-all(bf16[32,5,2048]{2,1,0:T(8,128)(2,1)S(1)} %get-tuple-element.6), channel_id=1, replica_groups=mesh['grp'=2,'sp'=32,'tp'=4] {'sp'}, dimensions={0} | all-to-all | bytes 1310720 | tf_op jit(solution)/shard_map/all_to_all | solution.py:49
  199.9 1.3 copy.47
  201.1 0.1 all-gather.7.cloned.1.call-update
  201.2 0.0 all-gather.5.cloned.1.call-done
  201.2 3.2 copy.46
  204.4 2.2 reshape_reshape.6
  206.6 7.7 %fusion.10 = f32[640,896]{1,0:T(8,128)} fusion(bf16[640,2048]{1,0:T(8,128)(2,1)} %reshape_reshape.6, bf16[1,2048,896]{2,1,0:T(8,128)(2,1)} %param.19), kind=kOutput, calls=%fused_computation.12 | convolution fusion | flops 2348810240 | bytes 8585216 | tf_op jit(solution)/shard_map/dot_general | solution.py:71
  214.3 11.1 %fusion.12 = bf16[640,2048]{1,0:T(8,128)(2,1)} fusion(bf16[1,896,2048]{2,1,0:T(8,128)(2,1)} %param.21, f32[640,896]{1,0:T(8,128)} %fusion.10, bf16[640,2048]{1,0:T(8,128)(2,1)S(1)} %copy-done.4, bf16[1,2048,896]{2,1,0:T(8,128)(2,1)} %param.20), kind=kOutput, calls=%fused_computation.14 | convolution fusion | flops 4702371840 | bytes 14876672 | tf_op jit(solution)/shard_map/dot_general | solution.py:74
  225.4 5.4 %concatenate.13 = bf16[32,4,1,5,2048]{4,3,1,0,2:T(8,128)(2,1)} reshape(bf16[640,2048]{1,0:T(8,128)(2,1)} %fusion.12) | data formatting | bytes 5242880 | tf_op jit(solution)/shard_map/concatenate | solution.py:54
  230.8 1.9 all-gather.7.cloned.1.call-done
  232.7 3.2 copy.48
  235.9 2.4 reshape_reshape.7
  238.3 7.2 %fusion.8 = f32[640,896]{1,0:T(8,128)} fusion(bf16[640,2048]{1,0:T(8,128)(2,1)} %reshape_reshape.7, bf16[1,2048,896]{2,1,0:T(8,128)(2,1)} %param.19), kind=kOutput, calls=%fused_computation.10 | convolution fusion | flops 2348810240 | bytes 8585216 | tf_op jit(solution)/shard_map/dot_general | solution.py:71
  245.6 11.0 %fusion.15 = bf16[640,2048]{1,0:T(8,128)(2,1)} fusion(bf16[1,896,2048]{2,1,0:T(8,128)(2,1)} %param.21, f32[640,896]{1,0:T(8,128)} %fusion.8, bf16[640,2048]{1,0:T(8,128)(2,1)S(1)} %copy-done.5, bf16[1,2048,896]{2,1,0:T(8,128)(2,1)} %param.20), kind=kOutput, calls=%fused_computation.15 | convolution fusion | flops 4702371840 | bytes 14876672 | tf_op jit(solution)/shard_map/dot_general | solution.py:74
  256.5 5.5 %concatenate.14 = bf16[32,4,1,5,2048]{4,3,1,0,2:T(8,128)(2,1)} reshape(bf16[640,2048]{1,0:T(8,128)(2,1)} %fusion.15) | data formatting | bytes 5242880 | tf_op jit(solution)/shard_map/concatenate | solution.py:54
  262.0 10.4 %maximum_bitcast_fusion = bf16[4,32,1,10,2048]{4,3,0,1,2:T(8,128)(2,1)} fusion(bf16[32,4,1,5,2048]{4,3,1,0,2:T(8,128)(2,1)} %concatenate.14, bf16[32,4,1,5,2048]{4,3,1,0,2:T(8,128)(2,1)} %concatenate.13), kind=kLoop, calls=%fused_computation.1 | loop fusion | flops 10485760 | bytes 10485760 | tf_op jit(solution)/shard_map/transpose | solution.py:59
  272.5 6.3 %copy.49 = bf16[4,32,1,10,2048]{4,1,3,2,0:T(8,128)(2,1)S(1)} copy(bf16[4,32,1,10,2048]{4,3,0,1,2:T(8,128)(2,1)} %maximum_bitcast_fusion) | data formatting | bytes 10485760 | tf_op jit(solution)/shard_map/transpose | solution.py:59
  278.7 62.9 %all_to_all.44 = bf16[4,32,1,10,2048]{4,1,3,2,0:T(8,128)(2,1)} all-to-all(bf16[4,32,1,10,2048]{4,1,3,2,0:T(8,128)(2,1)S(1)} %copy.49), channel_id=1, replica_groups=mesh['grp'=2,'sp'=32,'tp'=4] {'tp'}, dimensions={0} | all-to-all | bytes 10485760 | tf_op jit(solution)/shard_map/all_to_all | solution.py:64
  341.6 3.6 reduce_sum.48
  345.2 2.1 copy.50
  347.3 14.5 %all-to-all-start.5 = ((bf16[32,1,10,2048]{3,2,1,0:T(8,128)(2,1)}), bf16[32,1,10,2048]{3,2,1,0:T(8,128)(2,1)}, u32[]{:S(2)}, u32[]{:S(2)}) async-start(bf16[32,1,10,2048]{3,2,1,0:T(8,128)(2,1)} %copy.50), calls=%async_computation.5 | async-start | bytes 4194304 | tf_op jit(solution)/shard_map/all_to_all | solution.py:151
  361.8 0.1 reduce_sum.46
  362.0 0.1 copy.51
  362.1 0.1 mul.98
  362.2 0.1 copy.43
  362.3 0.1 copy.44
  362.5 0.1 copy.52
  362.6 97.9 %all-to-all-done.5 = bf16[32,1,10,2048]{3,2,1,0:T(8,128)(2,1)} async-done(((bf16[32,1,10,2048]{3,2,1,0:T(8,128)(2,1)}), bf16[32,1,10,2048]{3,2,1,0:T(8,128)(2,1)}, u32[]{:S(2)}, u32[]{:S(2)}) %all-to-all-start.5) | async-done | bytes 1310752 | tf_op jit(solution)/shard_map/all_to_all | solution.py:151
  460.5 2.5 reshape.125
  463.0 2.7 gather_fusion
  465.7 2.5 gather.7
  468.2 4.2 multiply_reduce_fusion
  472.5 0.9 add_convert_fusion
  (30 shorter events, 0.1 us)
Async XLA Ops:
  6.5 24.0 %copy-start = (bf16[1,128,128]{2,1,0:T(8,128)(2,1)S(1)}, bf16[1,128,128]{2,1,0:T(8,128)(2,1)}, u32[]{:S(2)}) copy-start(bf16[1,128,128]{2,1,0:T(8,128)(2,1)} %param.13) | copy-start | bytes 98308
  7.2 22.4 %collective-permute-start = (bf16[15,128]{1,0:T(8,128)(2,1)S(1)}, bf16[15,128]{1,0:T(8,128)(2,1)S(1)}, u32[]{:S(2)}, u32[]{:S(2)}) collective-permute-start(bf16[15,128]{1,0:T(8,128)(2,1)S(1)} %slice.64), channel_id=1, source_target_pairs={{0,4},{4,8},{8,12},{12,16},{16,20},{20,24},{24,28},{28,32},{32,36}... | collective-permute-start | bytes 11528 | tf_op jit(solution)/shard_map/ppermute | solution.py:15
  30.5 8.1 %copy-start.6 = (bf16[128,2048]{1,0:T(8,128)(2,1)S(1)}, bf16[128,2048]{1,0:T(8,128)(2,1)}, u32[]{:S(2)}) copy-start(bf16[128,2048]{1,0:T(8,128)(2,1)} %param.15) | copy-start | bytes 1572868
  40.2 3.9 copy-start.8
  40.2 4.3 copy-start.9
  40.2 28.9 %copy-start.7 = (bf16[128,2048]{1,0:T(8,128)(2,1)S(1)}, bf16[128,2048]{1,0:T(8,128)(2,1)}, u32[]{:S(2)}) copy-start(bf16[128,2048]{1,0:T(8,128)(2,1)} %param.11) | copy-start | bytes 1572868
  40.2 28.9 %all-to-all-start.1 = ((bf16[4,128,2048]{2,1,0:T(8,128)(2,1)}), bf16[4,128,2048]{2,1,0:T(8,128)(2,1)S(1)}, u32[]{:S(2)}, u32[]{:S(2)}) async-start(bf16[4,128,2048]{2,1,0:T(8,128)(2,1)} %broadcast_in_dim.53), calls=%async_computation.1 | async-start | bytes 4194304 | tf_op jit(solution)/shard_map/all_to_all | solution.py:20
  44.0 157.2 %all-gather.5.cloned.1.call-start = ((), (), s32[]{:S(2)}) async-start(), calls=%async_computation.6 | async-start | bytes 3276800 | tf_op jit(solution)/shard_map/all_gather | solution.py:143
  69.6 1.0 copy-start.2
  140.6 92.1 %all-gather.7.cloned.1.call-start = ((), (), s32[]{:S(2)}) async-start(), calls=%async_computation.7 | async-start | bytes 3276800 | tf_op jit(solution)/shard_map/all_gather | solution.py:143
  206.6 7.7 %copy-start.4 = (bf16[640,2048]{1,0:T(8,128)(2,1)S(1)}, bf16[640,2048]{1,0:T(8,128)(2,1)}, u32[]{:S(2)}) copy-start(bf16[640,2048]{1,0:T(8,128)(2,1)} %reshape_reshape.6) | copy-start | bytes 7864324
  238.3 7.3 %copy-start.5 = (bf16[640,2048]{1,0:T(8,128)(2,1)S(1)}, bf16[640,2048]{1,0:T(8,128)(2,1)}, u32[]{:S(2)}) copy-start(bf16[640,2048]{1,0:T(8,128)(2,1)} %reshape_reshape.7) | copy-start | bytes 7864324
  347.3 15.1 %copy-start.10 = (f32[128,2]{0,1:T(2,128)S(1)}, f32[128,2]{0,1:T(2,128)}, u32[]{:S(2)}) copy-start(f32[128,2]{0,1:T(2,128)} %param.18) | copy-start | bytes 3076
  347.3 113.2 %all-to-all-start.5 = ((bf16[32,1,10,2048]{3,2,1,0:T(8,128)(2,1)}), bf16[32,1,10,2048]{3,2,1,0:T(8,128)(2,1)}, u32[]{:S(2)}, u32[]{:S(2)}) async-start(bf16[32,1,10,2048]{3,2,1,0:T(8,128)(2,1)} %copy.50), calls=%async_computation.5 | async-start | bytes 4194304 | tf_op jit(solution)/shard_map/all_to_all | solution.py:151
  465.7 7.7 %copy-start.1 = (bf16[1,128,128]{2,1,0:T(8,128)(2,1)S(1)}, bf16[1,128,128]{2,1,0:T(8,128)(2,1)}, u32[]{:S(2)}) copy-start(bf16[1,128,128]{2,1,0:T(8,128)(2,1)} %param.13) | copy-start | bytes 98308
  468.2 4.2 copy-start.3
Sparse Core Ops, SparseCore 0:
  140.7 31.4 all-gather.4
  201.3 31.3 all-gather.6
where the time goes:
time: 487 us; the launch traced here: 481 us
  blocking collectives  195 us (40%)
  waiting for transfers between devices  139 us (29%)
  local copies, waits for them, and re-layouts  47.1 us (10%)
  matrix products  38.7 us (8%)
  starting transfers between devices  24.2 us (5%)
  other arithmetic  21.7 us (4%)
  between operations  14.2 us (3%)
    all_to_all x2, blocking collectives, grouped_exchange(): lax.all_to_all(group, axis, split_axis=split_dim, concat_axis=concat_dim,...  125 us
    all_to_all x1, waiting for transfers between devices, local(): lax.all_to_all(route_sums.astype(jnp.bfloat16), 'sp', split_axis=0, conca...  97.9 us
    all_to_all x1, blocking collectives, sent_and_summed(): tiles = lax.all_to_all(split_up(value, dim, count), axis, 0, 0, tiled=True)  62.9 us
    all_to_all x1, waiting for transfers between devices, copy_for_each(): lax.all_to_all(jnp.broadcast_to(value[None], (count, *value.shape)), axis...  23.6 us
    dot_general x2, matrix products, expert_block(): jnp.dot(hidden, down_w, preferred_element_type=jnp.float32)  22 us
    ppermute x1, waiting for transfers between devices, from_behind(): lax.ppermute(value, axis, [(source, source + steps) for source in range(l...  15.9 us
    dot_general x2, matrix products, expert_block(): gate = jnp.dot(flat, gate_w, preferred_element_type=jnp.float32)  14.9 us
    all_to_all x1, starting transfers between devices, local(): lax.all_to_all(route_sums.astype(jnp.bfloat16), 'sp', split_axis=0, conca...  14.5 us
  transfers between devices with their start and end apart: 5, of which 4 were waited for; matrix products, arithmetic and copies ran while one was open for 7% of the time, Pallas kernels for 0%

commit v1 on v0

v1 whole, which is shorter than its diff:
```python
import functools

import jax
import jax.numpy as jnp
from jax import lax
from jax.experimental import pallas as pl
from jax.experimental.pallas import tpu as pltpu
from jax.sharding import PartitionSpec as P

MESH = pl.DeviceIdType.MESH
BF16 = jnp.bfloat16
F32 = jnp.float32
I32 = jnp.int32

norm_eps = 1e-06
PAIR = 2
SEG = 256
HALO = 16


def iota(shape, dim):
    return lax.broadcasted_iota(I32, shape, dim)


def dot(a, b):
    return jnp.dot(a, b, preferred_element_type=F32)


def settle(like, sem):
    pltpu.make_async_copy(like, like, sem).wait()


def kernel(
    sizes,
    resid_ref,
    pool_ref,
    map_ref,
    scale_ref,
    proj_ref,
    gain_ref,
    routes_ref,
    weight_ref,
    gate_hbm,
    up_hbm,
    down_hbm,
    out_ref,
    ext,
    halo,
    pieces,
    piece_in,
    proj_in,
    mixed,
    spread,
    gather,
    w_hi,
    w_lo,
    w_gu,
    w_down,
    stack,
    go,
    came,
    rows,
    hidden,
    part,
    part_in,
    back,
    home,
    total,
    w_sem,
    halo_sem,
    proj_send,
    proj_recv,
    mate_send,
    mate_recv,
    piece_send,
    piece_recv,
    go_send,
    go_recv,
    row_send,
    row_recv,
    part_send,
    part_recv,
    back_send,
    back_recv,
):
    n, lanes, chunks, slots = sizes
    tokens, width = resid_ref.shape
    seq_rows, gdim = pool_ref.shape
    segs = width // SEG
    block = PAIR * segs
    crows = PAIR * n
    half = gdim // 2
    me = lax.axis_index("sp")
    lane = lax.axis_index("tp")
    core = lax.rem(me, 2)
    mate = me + 1 - 2 * core

    def sp_at(k):
        return lax.rem(me + k, n)

    def tp_at(k):
        return lax.rem(lane + k, lanes)

    def remote(src, dst, send, recv, where):
        return pltpu.make_async_remote_copy(
            src_ref=src,
            dst_ref=dst,
            send_sem=send,
            recv_sem=recv,
            device_id=where,
            device_id_type=MESH,
        )

    barrier = pltpu.get_barrier_semaphore()

    def greet(k, carry):
        pl.semaphore_signal(
            barrier, inc=1, device_id={"sp": sp_at(k)}, device_id_type=MESH
        )
        return carry

    lax.fori_loop(1, n, greet, 0)
    for k in range(1, lanes):
        pl.semaphore_signal(
            barrier, inc=1, device_id={"tp": tp_at(k)}, device_id_type=MESH
        )

    size = n * block
    a, b = iota((size, size), 0), iota((size, size), 1)
    seg_a, rest = a // crows, lax.rem(a, crows)
    where = (rest // PAIR) * block + seg_a * PAIR + lax.rem(rest, PAIR)
    gather[...] = (b == where).astype(F32).astype(BF16)
    seg_b, rest_b = b // crows, lax.rem(b, crows)
    where_b = (rest_b // PAIR) * block + seg_b * PAIR + lax.rem(rest_b, PAIR)
    spread[...] = (a == where_b).astype(F32).astype(BF16)

    one0 = (iota((n, tokens), 0) == routes_ref[0:1, :]).astype(F32)
    one1 = (iota((n, tokens), 0) == routes_ref[1:2, :]).astype(F32)
    before = (iota((tokens, tokens), 0) < iota((tokens, tokens), 1)).astype(F32).astype(BF16)
    rank0 = dot(one0.astype(BF16), before)
    rank1 = dot(one1.astype(BF16), before) + jnp.sum(one0, axis=1, keepdims=True)
    slot0 = jnp.sum(rank0 * one0, axis=0, keepdims=True).astype(I32)
    slot1 = jnp.sum(rank1 * one1, axis=0, keepdims=True).astype(I32)
    row0 = (slot0 // PAIR) * crows + routes_ref[0:1, :] * PAIR + lax.rem(slot0, PAIR)
    row1 = (slot1 // PAIR) * crows + routes_ref[1:2, :] * PAIR + lax.rem(slot1, PAIR)
    place = iota((chunks * crows, tokens), 0)
    hit0, hit1 = place == row0, place == row1
    weight = jnp.where(hit0, weight_ref[0:1, :], 0.0) + jnp.where(hit1, weight_ref[1:2, :], 0.0)
    high = weight.astype(BF16)
    w_hi[...] = high.reshape(chunks, crows, tokens)
    w_lo[...] = (weight - high.astype(F32)).astype(BF16).reshape(chunks, crows, tokens)
    placing = (jnp.where(hit0, 1.0, 0.0) + jnp.where(hit1, 1.0, 0.0)).astype(BF16)

    pl.semaphore_wait(barrier, n - 1 + lanes - 1)

    halo_copy = remote(
        pool_ref.at[pl.ds(seq_rows - HALO, HALO)],
        halo,
        halo_sem.at[0],
        halo_sem.at[1],
        {"sp": sp_at(1)},
    )
    halo_copy.start()
    mine = pl.ds(pl.multiple_of(core * half, half), half)
    other = pl.ds(pl.multiple_of((1 - core) * half, half), half)

    def proj_copy(k):
        return remote(
            proj_ref.at[mine],
            proj_in.at[k - 1, mine],
            proj_send.at[k - 1],
            proj_recv.at[k - 1],
            {"tp": tp_at(k)},
        )

    def mate_copy(k):
        return remote(
            proj_in.at[k - 1, mine],
            proj_in.at[k - 1, mine],
            mate_send.at[k - 1],
            mate_recv.at[k - 1],
            {"sp": mate},
        )

    order = [k for k in (1, 3, 2) if k < lanes]
    for k in order:
        proj_copy(k).start()

    tiles = w_gu.shape[0]
    cols = w_down.shape[0]
    tile = w_gu.shape[2] // 2

    def weight_copies():
        found = []
        for i in range(tiles):
            for j, source in enumerate((gate_hbm, up_hbm)):
                found.append(
                    pltpu.make_async_copy(
                        source.at[0, :, pl.ds(i * tile, tile)],
                        w_gu.at[i, :, pl.ds(j * tile, tile)],
                        w_sem.at[j * tiles + i],
                    )
                )
        for i in range(cols):
            found.append(
                pltpu.make_async_copy(
                    down_hbm.at[0, :, pl.ds(i * SEG, SEG)], w_down.at[i], w_sem.at[2 * tiles + i]
                )
            )
        return found

    for copy in weight_copies():
        copy.start()

    ext[pl.ds(HALO, seq_rows)] = pool_ref[...].astype(F32)
    halo_copy.wait()
    ext[pl.ds(0, HALO)] = jnp.where(me > 0, halo[...].astype(F32), 0.0)
    span = seq_rows + HALO
    levels = []
    reach = 1
    for level in range(lanes):
        kept = ext[pl.ds(0, span)]
        ext[pl.ds(reach, span - reach)] = kept[reach:] + kept[: span - reach]
        levels.append(ext[pl.ds(HALO, seq_rows)])
        reach *= 2
    window_sum = levels[0]
    for level in range(1, lanes):
        window_sum = jnp.where(lane == level, levels[level], window_sum)
    window = jnp.left_shift(jnp.int32(2), lane)
    positions = me * seq_rows + 1 + iota((seq_rows, gdim), 0)
    divisor = jnp.minimum(positions, window).astype(F32)
    pooled = (window_sum / divisor - pool_ref[...].astype(F32)).astype(BF16)
    pieces[...] = (dot(pooled, map_ref[0]) * scale_ref[...].astype(F32)).astype(BF16)

    def piece_copy(k):
        return remote(
            pieces.at[pl.ds(pl.multiple_of(tp_at(k) * tokens, tokens), tokens)],
            piece_in.at[k - 1],
            piece_send.at[k - 1],
            piece_recv.at[k - 1],
            {"tp": tp_at(k)},
        )

    for k in order:
        piece_copy(k).start()
    mix = dot(pieces[pl.ds(pl.multiple_of(lane * tokens, tokens), tokens)], proj_ref[...])
    for k in order:
        proj_copy(k).wait_recv()
        mate_copy(k).start()
    for k in order:
        piece_copy(k).wait_recv()
        settle(proj_in.at[k - 1, other], mate_recv.at[k - 1])
        mix = mix + dot(piece_in[k - 1], proj_in[k - 1])
    mixed_value = (resid_ref[...].astype(F32) + mix).astype(BF16)
    mixed[...] = mixed_value
    residual = mixed_value.astype(F32)
    scaled = residual * lax.rsqrt(
        jnp.sum(residual * residual, axis=1, keepdims=True) / width + norm_eps
    )
    normed = (scaled * gain_ref[...].astype(F32)).astype(BF16)
    routed = dot(placing, normed).astype(BF16)
    total[...] = residual

    def to_blocks(value, target):
        for s in range(segs):
            stack[pl.ds(s * crows, crows)] = value[:, s * SEG : (s + 1) * SEG]
        target[...] = dot(spread[...], stack[...]).astype(BF16)

    for c in range(chunks):
        to_blocks(routed[c * crows : (c + 1) * crows], go.at[c])

    def send_blocks(source, target, c, send, recv):
        own = pl.ds(pl.multiple_of(me * block, block), block)

        def one(k, carry):
            to = sp_at(k)
            remote(
                source.at[c, pl.ds(pl.multiple_of(to * block, block), block)],
                target.at[c, own],
                send.at[c],
                recv.at[c],
                {"sp": to},
            ).start()
            return carry

        def both(k, carry):
            one(k, 0)
            one(n - k, 0)
            return carry

        lax.fori_loop(1, n // 2, both, 0)
        one(n // 2, 0)

    def take_blocks(source, target, c, recv):
        own = pl.ds(pl.multiple_of(me * block, block), block)
        settle(target.at[c, pl.ds(0, (n - 1) * block)], recv.at[c])
        target[c, own] = source[c, own]
        return dot(gather[...], target[c]).astype(BF16)

    def row_copy(c, k):
        own = pl.ds(pl.multiple_of(lane * crows, crows), crows)
        return remote(
            rows.at[c, own],
            rows.at[c, own],
            row_send.at[c, k - 1],
            row_recv.at[c, k - 1],
            {"tp": tp_at(k)},
        )

    def part_copy(c, k):
        theirs = pl.ds(pl.multiple_of(tp_at(k) * crows, crows), crows)
        return remote(
            part.at[c, theirs],
            part_in.at[c, k - 1],
            part_send.at[c, k - 1],
            part_recv.at[c, k - 1],
            {"tp": tp_at(k)},
        )

    ahead = min(2, chunks)
    for c in range(ahead):
        send_blocks(go, came, c, go_send, go_recv)
    for copy in weight_copies():
        copy.wait()

    def step(k, carry):
        @pl.when(k < chunks)
        def _():
            flat = take_blocks(go, came, k, go_recv)
            own = pl.ds(pl.multiple_of(lane * crows, crows), crows)
            for s in range(segs):
                rows[k, own, s * SEG : (s + 1) * SEG] = flat[s * crows : (s + 1) * crows]
            for j in order:
                row_copy(k, j).start()

            @pl.when(k + ahead < chunks)
            def _():
                send_blocks(go, came, k + ahead, go_send, go_recv)

        @pl.when((k >= 1) & (k < chunks + 1))
        def _():
            c = k - 1
            for j in order:
                row_copy(c, j).wait_recv()

            def up_tile(i, carry):
                both = dot(rows[c], w_gu[i])
                g, u = both[:, :tile], both[:, tile:]
                hidden[:, pl.ds(pl.multiple_of(i * tile, tile), tile)] = (
                    (g / (1.0 + jnp.exp(-g))) * u
                ).astype(BF16)
                return carry

            lax.fori_loop(0, tiles, up_tile, 0)

            def down_tile(i, carry):
                part[c, :, pl.ds(pl.multiple_of(i * SEG, SEG), SEG)] = dot(
                    hidden[...], w_down[i]
                ).astype(BF16)
                return carry

            lax.fori_loop(0, cols, down_tile, 0)
            for j in order:
                part_copy(c, j).start()

        @pl.when((k >= 2) & (k < chunks + 2))
        def _():
            c = k - 2
            own = pl.ds(pl.multiple_of(lane * crows, crows), crows)
            for j in order:
                part_copy(c, j).wait_recv()
            value = part[c, own].astype(F32)
            for j in order:
                value = value + part_in[c, j - 1].astype(F32)
            to_blocks(value.astype(BF16), back.at[c])
            send_blocks(back, home, c, back_send, back_recv)

        @pl.when(k >= 3)
        def _():
            c = k - 3
            flat = take_blocks(back, home, c, back_recv)
            sides = (((0,), (0,)), ((), ()))
            for s in range(segs):
                piece = flat[s * crows : (s + 1) * crows]
                cut = pl.ds(s * SEG, SEG)
                total[:, cut] += lax.dot_general(
                    w_hi[c], piece, sides, preferred_element_type=F32
                ) + lax.dot_general(w_lo[c], piece, sides, preferred_element_type=F32)

        return carry

    lax.fori_loop(0, chunks + 3, step, 0)
    out_ref[...] = total[...].astype(BF16)

    for k in order:
        proj_copy(k).wait_send()
        mate_copy(k).wait_send()
        piece_copy(k).wait_send()

    def drain(c, carry):
        settle(go.at[c, pl.ds(0, (n - 1) * block)], go_send.at[c])
        settle(back.at[c, pl.ds(0, (n - 1) * block)], back_send.at[c])
        for k in order:
            row_copy(c, k).wait_send()
            part_copy(c, k).wait_send()
        return carry

    lax.fori_loop(0, chunks, drain, 0)


def local(
    resid,
    pool_input,
    group_map,
    pool_scale,
    out_proj,
    norm_gain,
    routes,
    route_weight,
    expert_gate,
    expert_up,
    expert_down,
):
    n, lanes = lax.axis_size("sp"), lax.axis_size("tp")
    tokens, width = resid.shape
    seq_rows, gdim = pool_input.shape
    ff = expert_gate.shape[2]
    slots = max(2, 5 * tokens * routes.shape[1] // (4 * n))
    chunks = slots // PAIR
    assert chunks * PAIR == slots
    segs = width // SEG
    size = n * PAIR * segs
    crows = PAIR * n
    tile = min(128, ff)
    tiles, cols = ff // tile, width // SEG
    vmem, dma = pltpu.VMEM, pltpu.SemaphoreType.DMA
    hbm = pl.BlockSpec(memory_space=pl.ANY)
    scratch = [
        vmem((HALO + seq_rows, gdim), F32),
        vmem((HALO, gdim), BF16),
        vmem((seq_rows, gdim), BF16),
        vmem((lanes - 1, tokens, gdim), BF16),
        vmem((lanes - 1, gdim, width), BF16),
        vmem((tokens, width), BF16),
        vmem((size, size), BF16),
        vmem((size, size), BF16),
        vmem((chunks, crows, tokens), BF16),
        vmem((chunks, crows, tokens), BF16),
        vmem((tiles, width, 2 * tile), BF16),
        vmem((cols, ff, SEG), BF16),
        vmem((size, SEG), BF16),
        vmem((chunks, size, SEG), BF16),
        vmem((chunks, size, SEG), BF16),
        vmem((chunks, lanes * crows, width), BF16),
        vmem((lanes * crows, ff), BF16),
        vmem((chunks, lanes * crows, width), BF16),
        vmem((chunks, lanes - 1, crows, width), BF16),
        vmem((chunks, size, SEG), BF16),
        vmem((chunks, size, SEG), BF16),
        vmem((tokens, width), F32),
        dma((2 * tiles + cols,)),
        dma((2,)),
        dma((lanes - 1,)),
        dma((lanes - 1,)),
        dma((lanes - 1,)),
        dma((lanes - 1,)),
        dma((lanes - 1,)),
        dma((lanes - 1,)),
        dma((chunks,)),
        dma((chunks,)),
        dma((chunks, lanes - 1)),
        dma((chunks, lanes - 1)),
        dma((chunks, lanes - 1)),
        dma((chunks, lanes - 1)),
        dma((chunks,)),
        dma((chunks,)),
    ]
    return pl.pallas_call(
        functools.partial(kernel, (n, lanes, chunks, slots)),
        out_shape=jax.ShapeDtypeStruct((tokens, width), BF16),
        in_specs=[pl.BlockSpec(memory_space=vmem)] * 8 + [hbm] * 3,
        out_specs=pl.BlockSpec(memory_space=vmem),
        scratch_shapes=scratch,
        compiler_params=pltpu.CompilerParams(
            collective_id=0, has_side_effects=True, vmem_limit_bytes=60 * 1024 * 1024
        ),
        name="layer",
    )(
        resid,
        pool_input,
        group_map,
        pool_scale.reshape(1, -1),
        out_proj,
        norm_gain.reshape(1, -1),
        routes.T,
        route_weight.T,
        expert_gate,
        expert_up,
        expert_down,
    )


def solution(mesh):
    return jax.shard_map(
        local,
        mesh=mesh,
        in_specs=(
            P(("grp", "sp", "tp"), None),
            P(("grp", "sp"), "tp"),
            P("tp", None, None),
            P("tp"),
            P("tp", None),
            P(),
            P(("grp", "sp", "tp"), None),
            P(("grp", "sp", "tp"), None),
            P("sp", None, "tp"),
            P("sp", None, "tp"),
            P("sp", "tp", None),
        ),
        out_specs=P(("grp", "sp", "tp"), None),
        check_vma=False,
    )
```

time: 487 us -> 202 us (0.41); the launches traced: 481 us -> 202 us
  Pallas kernels: 0 us -> 198 us
  blocking collectives: 195 us -> 0 us
  waiting for transfers between devices: 139 us -> 0 us
  local copies, waits for them, and re-layouts: 47.1 us -> 3.17 us
  matrix products: 38.7 us -> 0 us
  starting transfers between devices: 24.2 us -> 0 us
  other arithmetic: 21.7 us -> 0 us
  between operations: 14.2 us -> 0.01 us
    pallas_call x0 -> x1, Pallas kernels: none -> 198 us  [local(): pl.pallas_call(functools.partial(kernel, (n, lanes, chunks, slots)), out_...]
    all_to_all x4 -> x0, blocking collectives: 195 us -> none  [the longest x2 125 us: grouped_exchange(): lax.all_to_all(group, axis, split_axis=split_dim, concat_axis=concat_dim,...]
    all_to_all x2 -> x0, waiting for transfers between devices: 122 us -> none  [the longest x1 97.9 us: local(): lax.all_to_all(route_sums.astype(jnp.bfloat16), 'sp', split_axis=0, conca...]
    dot_general x7 -> x0, matrix products: 38.7 us -> none  [the longest x2 22 us: expert_block(): jnp.dot(hidden, down_w, preferred_element_type=jnp.float32)]
    all_to_all x2 -> x0, starting transfers between devices: 18.3 us -> none  [the longest x1 14.5 us: local(): lax.all_to_all(route_sums.astype(jnp.bfloat16), 'sp', split_axis=0, conca...]
    ppermute x1 -> x0, waiting for transfers between devices: 15.9 us -> none  [from_behind(): lax.ppermute(value, axis, [(source, source + steps) for source in range(l...]
    concatenate x2 -> x0, local copies, waits for them, and re-layouts: 10.9 us -> none  [grouped_exchange(): jnp.concatenate(parts, axis=out_dim)]
    transpose x1 -> x0, other arithmetic: 10.4 us -> none  [split_up(): return jnp.moveaxis(value.reshape(*before, count, -1, *after), dim, 0)]
  transfers between devices with their start and end apart: 5 -> 0, of which waited for: 4 -> 0; matrix products, arithmetic and copies ran while one was open for 7% -> 0% of each run, Pallas kernels for 0% -> 0%
where the time goes in v1:
time: 202 us
  Pallas kernels  198 us (98%)
  local copies, waits for them, and re-layouts  3.17 us (2%)
    pallas_call x1, Pallas kernels, local(): pl.pallas_call(functools.partial(kernel, (n, lanes, chunks, slots)), out_...  198 us

profile of v1, /device:TPU:33, one launch (start us, length us, event | category | flops | bytes accessed | tf_op | source)
XLA Modules:
  0.0 201.6 jit_solution(1972165831165449128)
XLA Ops:
  0.0 1.3 reshape.7.gain_ref
  1.3 198.4 %layer.1 = bf16[128,2048]{1,0:T(8,128)(2,1)} custom-call(bf16[128,2048]{1,0:T(8,128)(2,1)} %resid_ref.1, bf16[512,128]{1,0:T(8,128)(2,1)} %pool_ref.1, bf16[1,128,128]{2,1,0:T(8,128)(2,1)} %map_ref.1, bf16[1,128]{1,0:T(2,128)(2,1)} %bitcast.5, bf16[128,2048]{1,0:T(8,128)(2,1)} %proj_ref.1, bf16[1,2048]{1,0:T(2,128)(2,1)} %reshape.7.gain_ref, ...), custom_call_target="tpu_custom_call" | custom-call | tf_op jit(solution)/shard_map/layer/pallas_call | solution.py:478
  199.7 1.9 copy.13

commit v2 on v1

--- a/solution.py
+++ b/solution.py
@@ -16,6 +16,17 @@
 PAIR = 2
 SEG = 256
 HALO = 16
+AHEAD = 2
+
+SCHEDULE = (
+    ("arrive", 0),
+    ("send_next", -AHEAD),
+    ("experts", 1),
+    ("relay", 0),
+    ("add_far", 1),
+    ("give_back", 2),
+    ("combine", 3),
+)
 
 
 def iota(shape, dim):
@@ -63,6 +74,7 @@
     hidden,
     part,
     part_in,
+    far_in,
     back,
     home,
     total,
@@ -297,99 +309,137 @@
         target[c, own] = source[c, own]
         return dot(gather[...], target[c]).astype(BF16)
 
-    def row_copy(c, k):
-        own = pl.ds(pl.multiple_of(lane * crows, crows), crows)
-        return remote(
-            rows.at[c, own],
-            rows.at[c, own],
-            row_send.at[c, k - 1],
-            row_recv.at[c, k - 1],
-            {"tp": tp_at(k)},
-        )
-
-    def part_copy(c, k):
-        theirs = pl.ds(pl.multiple_of(tp_at(k) * crows, crows), crows)
-        return remote(
-            part.at[c, theirs],
-            part_in.at[c, k - 1],
-            part_send.at[c, k - 1],
-            part_recv.at[c, k - 1],
-            {"tp": tp_at(k)},
-        )
-
-    ahead = min(2, chunks)
+    right, left = {"tp": tp_at(1)}, {"tp": tp_at(lanes - 1)}
+    low = crows // 2
+
+    def of_lane(k, start, count):
+        return pl.ds(pl.multiple_of(tp_at(k) * crows + start, low), count)
+
+    def row_copies(c):
+        def one(k, start, i, to):
+            at = rows.at[c, of_lane(k, start, low)]
+            return remote(at, at, row_send.at[c, i], row_recv.at[c, i], to)
+
+        return (
+            one(0, 0, 0, right),
+            one(0, low, 1, left),
+            one(0, low, 2, right),
+            one(0, 0, 3, left),
+            one(lanes - 1, 0, 4, right),
+            one(1, low, 5, left),
+        )
+
+    def part_copies(c):
+        def one(k, start, target, i, to):
+            at = part.at[c, of_lane(k, start, low)]
+            return remote(at, target, part_send.at[c, i], part_recv.at[c, i], to)
+
+        return (
+            one(2, 0, far_in.at[c, 0], 0, right),
+            one(2, low, far_in.at[c, 1], 1, left),
+            one(1, low, part_in.at[c, 0, pl.ds(low, low)], 2, right),
+            one(lanes - 1, 0, part_in.at[c, 1, pl.ds(0, low)], 3, left),
+            one(1, 0, part_in.at[c, 0, pl.ds(0, low)], 4, right),
+            one(lanes - 1, low, part_in.at[c, 1, pl.ds(low, low)], 5, left),
+        )
+
+    ahead = min(AHEAD, chunks)
     for c in range(ahead):
         send_blocks(go, came, c, go_send, go_recv)
     for copy in weight_copies():
         copy.wait()
 
+    def arrive(c):
+        flat = take_blocks(go, came, c, go_recv)
+        own = of_lane(0, 0, crows)
+        for s in range(segs):
+            rows[c, own, s * SEG : (s + 1) * SEG] = flat[s * crows : (s + 1) * crows]
+        for copy in row_copies(c)[:4]:
+            copy.start()
+
+    def relay(c):
+        copies = row_copies(c)
+        for i in (0, 1):
+            copies[i].wait_recv()
+            copies[4 + i].start()
+
+    def experts(c):
+        copies = row_copies(c)
+        for i in (2, 3, 4, 5):
+            copies[i].wait_recv()
+
+        def up_tile(i, carry):
+            both = dot(rows[c], w_gu[i])
+            g, u = both[:, :tile], both[:, tile:]
+            hidden[:, pl.ds(pl.multiple_of(i * tile, tile), tile)] = (
+                (g / (1.0 + jnp.exp(-g))) * u
+            ).astype(BF16)
+            return carry
+
+        lax.fori_loop(0, tiles, up_tile, 0)
+
+        def down_tile(i, carry):
+            part[c, :, pl.ds(pl.multiple_of(i * SEG, SEG), SEG)] = dot(
+                hidden[...], w_down[i]
+            ).astype(BF16)
+            return carry
+
+        lax.fori_loop(0, cols, down_tile, 0)
+        for copy in part_copies(c)[:4]:
+            copy.start()
+
+    def add_far(c):
+        copies = part_copies(c)
+        for i, (k, start) in enumerate(((1, 0), (lanes - 1, low))):
+            copies[i].wait_recv()
+            at = of_lane(k, start, low)
+            part[c, at] = (part[c, at].astype(F32) + far_in[c, i].astype(F32)).astype(BF16)
+            copies[4 + i].start()
+
+    def give_back(c):
+        copies = part_copies(c)
+        for i in (2, 3, 4, 5):
+            copies[i].wait_recv()
+        value = part[c, of_lane(0, 0, crows)].astype(F32)
+        value = value + part_in[c, 0].astype(F32) + part_in[c, 1].astype(F32)
+        to_blocks(value.astype(BF16), back.at[c])
+        send_blocks(back, home, c, back_send, back_recv)
+
+    def combine(c):
+        flat = take_blocks(back, home, c, back_recv)
+        sides = (((0,), (0,)), ((), ()))
+        for s in range(segs):
+            piece = flat[s * crows : (s + 1) * crows]
+            cut = pl.ds(s * SEG, SEG)
+            total[:, cut] += lax.dot_general(
+                w_hi[c], piece, sides, preferred_element_type=F32
+            ) + lax.dot_general(w_lo[c], piece, sides, preferred_element_type=F32)
+
+    def send_next(c):
+        send_blocks(go, came, c, go_send, go_recv)
+
+    stages = {
+        "arrive": arrive,
+        "relay": relay,
+        "experts": experts,
+        "add_far": add_far,
+        "give_back": give_back,
+        "combine": combine,
+        "send_next": send_next,
+    }
+
     def step(k, carry):
-        @pl.when(k < chunks)
-        def _():
-            flat = take_blocks(go, came, k, go_recv)
-            own = pl.ds(pl.multiple_of(lane * crows, crows), crows)
-            for s in range(segs):
-                rows[k, own, s * SEG : (s + 1) * SEG] = flat[s * crows : (s + 1) * crows]
-            for j in order:
-                row_copy(k, j).start()
-
-            @pl.when(k + ahead < chunks)
+        for name, lag in SCHEDULE:
+            c = k - lag
+            low_end = ahead if name == "send_next" else 0
+
+            @pl.when((c >= low_end) & (c < chunks))
             def _():
-                send_blocks(go, came, k + ahead, go_send, go_recv)
-
-        @pl.when((k >= 1) & (k < chunks + 1))
-        def _():
-            c = k - 1
-            for j in order:
-                row_copy(c, j).wait_recv()
-
-            def up_tile(i, carry):
-                both = dot(rows[c], w_gu[i])
-                g, u = both[:, :tile], both[:, tile:]
-                hidden[:, pl.ds(pl.multiple_of(i * tile, tile), tile)] = (
-                    (g / (1.0 + jnp.exp(-g))) * u
-                ).astype(BF16)
-                return carry
-
-            lax.fori_loop(0, tiles, up_tile, 0)
-
-            def down_tile(i, carry):
-                part[c, :, pl.ds(pl.multiple_of(i * SEG, SEG), SEG)] = dot(
-                    hidden[...], w_down[i]
-                ).astype(BF16)
-                return carry
-
-            lax.fori_loop(0, cols, down_tile, 0)
-            for j in order:
-                part_copy(c, j).start()
-
-        @pl.when((k >= 2) & (k < chunks + 2))
-        def _():
-            c = k - 2
-            own = pl.ds(pl.multiple_of(lane * crows, crows), crows)
-            for j in order:
-                part_copy(c, j).wait_recv()
-            value = part[c, own].astype(F32)
-            for j in order:
-                value = value + part_in[c, j - 1].astype(F32)
-            to_blocks(value.astype(BF16), back.at[c])
-            send_blocks(back, home, c, back_send, back_recv)
-
-        @pl.when(k >= 3)
-        def _():
-            c = k - 3
-            flat = take_blocks(back, home, c, back_recv)
-            sides = (((0,), (0,)), ((), ()))
-            for s in range(segs):
-                piece = flat[s * crows : (s + 1) * crows]
-                cut = pl.ds(s * SEG, SEG)
-                total[:, cut] += lax.dot_general(
-                    w_hi[c], piece, sides, preferred_element_type=F32
-                ) + lax.dot_general(w_lo[c], piece, sides, preferred_element_type=F32)
+                stages[name](c)
 
         return carry
 
-    lax.fori_loop(0, chunks + 3, step, 0)
+    lax.fori_loop(0, chunks + max(lag for _, lag in SCHEDULE), step, 0)
     out_ref[...] = total[...].astype(BF16)
 
     for k in order:
@@ -400,9 +450,8 @@
     def drain(c, carry):
         settle(go.at[c, pl.ds(0, (n - 1) * block)], go_send.at[c])
         settle(back.at[c, pl.ds(0, (n - 1) * block)], back_send.at[c])
-        for k in order:
-            row_copy(c, k).wait_send()
-            part_copy(c, k).wait_send()
+        for copy in row_copies(c) + part_copies(c):
+            copy.wait_send()
         return carry
 
     lax.fori_loop(0, chunks, drain, 0)
@@ -427,7 +476,7 @@
     ff = expert_gate.shape[2]
     slots = max(2, 5 * tokens * routes.shape[1] // (4 * n))
     chunks = slots // PAIR
-    assert chunks * PAIR == slots
+    assert chunks * PAIR == slots and lanes == 4
     segs = width // SEG
     size = n * PAIR * segs
     crows = PAIR * n
@@ -454,7 +503,8 @@
         vmem((chunks, lanes * crows, width), BF16),
         vmem((lanes * crows, ff), BF16),
         vmem((chunks, lanes * crows, width), BF16),
-        vmem((chunks, lanes - 1, crows, width), BF16),
+        vmem((chunks, 2, crows, width), BF16),
+        vmem((chunks, 2, crows // 2, width), BF16),
         vmem((chunks, size, SEG), BF16),
         vmem((chunks, size, SEG), BF16),
         vmem((tokens, width), F32),
@@ -468,10 +518,10 @@
         dma((lanes - 1,)),
         dma((chunks,)),
         dma((chunks,)),
-        dma((chunks, lanes - 1)),
-        dma((chunks, lanes - 1)),
-        dma((chunks, lanes - 1)),
-        dma((chunks, lanes - 1)),
+        dma((chunks, 6)),
+        dma((chunks, 6)),
+        dma((chunks, 6)),
+        dma((chunks, 6)),
         dma((chunks,)),
         dma((chunks,)),
     ]

time: 202 us -> 185 us (0.916)
  Pallas kernels: 198 us -> 181 us
    pallas_call x1, Pallas kernels: 198 us -> 181 us  [local(): pl.pallas_call(functools.partial(kernel, (n, lanes, chunks, slots)), out_...]
where the time goes in v2:
time: 185 us; the launch traced here: 184 us
  Pallas kernels  181 us (98%)
  local copies, waits for them, and re-layouts  3.17 us (2%)
    pallas_call x1, Pallas kernels, local(): pl.pallas_call(functools.partial(kernel, (n, lanes, chunks, slots)), out_...  181 us

profile of v2, /device:TPU:33, one launch (start us, length us, event | category | flops | bytes accessed | tf_op | source)
XLA Modules:
  0.0 184.4 jit_solution(14255441620830006536)
XLA Ops:
  0.0 1.3 reshape.7.gain_ref
  1.3 181.2 %layer.1 = bf16[128,2048]{1,0:T(8,128)(2,1)} custom-call(bf16[128,2048]{1,0:T(8,128)(2,1)} %resid_ref.1, bf16[512,128]{1,0:T(8,128)(2,1)} %pool_ref.1, bf16[1,128,128]{2,1,0:T(8,128)(2,1)} %map_ref.1, bf16[1,128]{1,0:T(2,128)(2,1)} %bitcast.5, bf16[128,2048]{1,0:T(8,128)(2,1)} %proj_ref.1, bf16[1,2048]{1,0:T(2,128)(2,1)} %reshape.7.gain_ref, ...), custom_call_target="tpu_custom_call" | custom-call | tf_op jit(solution)/shard_map/layer/pallas_call | solution.py:528
  182.5 1.9 %copy.13 = bf16[128,2048]{1,0:T(8,128)(2,1)} copy(bf16[128,2048]{1,0:T(8,128)(2,1)} %layer.1) | data formatting | bytes 1048576

commit v3 on v2

--- a/solution.py
+++ b/solution.py
@@ -78,6 +78,7 @@
     back,
     home,
     total,
+    known,
     w_sem,
     halo_sem,
     proj_send,
@@ -125,13 +126,13 @@
 
     barrier = pltpu.get_barrier_semaphore()
 
-    def greet(k, carry):
-        pl.semaphore_signal(
-            barrier, inc=1, device_id={"sp": sp_at(k)}, device_id_type=MESH
-        )
-        return carry
-
-    lax.fori_loop(1, n, greet, 0)
+    def greet(sem, radius):
+        for k in (radius, n - radius):
+            pl.semaphore_signal(
+                sem, inc=1, device_id={"sp": sp_at(k)}, device_id_type=MESH
+            )
+
+    greet(barrier, 1)
     for k in range(1, lanes):
         pl.semaphore_signal(
             barrier, inc=1, device_id={"tp": tp_at(k)}, device_id_type=MESH
@@ -163,7 +164,7 @@
     w_lo[...] = (weight - high.astype(F32)).astype(BF16).reshape(chunks, crows, tokens)
     placing = (jnp.where(hit0, 1.0, 0.0) + jnp.where(hit1, 1.0, 0.0)).astype(BF16)
 
-    pl.semaphore_wait(barrier, n - 1 + lanes - 1)
+    pl.semaphore_wait(barrier, 2 + lanes - 1)
 
     halo_copy = remote(
         pool_ref.at[pl.ds(seq_rows - HALO, HALO)],
@@ -197,6 +198,12 @@
     order = [k for k in (1, 3, 2) if k < lanes]
     for k in order:
         proj_copy(k).start()
+
+    radius, level = 1, 0
+    while radius < n // 2:
+        greet(known.at[level], radius)
+        pl.semaphore_wait(known.at[level], 2)
+        radius, level = 2 * radius, level + 1
 
     tiles = w_gu.shape[0]
     cols = w_down.shape[0]
@@ -269,7 +276,16 @@
     scaled = residual * lax.rsqrt(
         jnp.sum(residual * residual, axis=1, keepdims=True) / width + norm_eps
     )
-    normed = (scaled * gain_ref[...].astype(F32)).astype(BF16)
+    unit = gain_ref.shape[1]
+    normed = jnp.concatenate(
+        [
+            (
+                scaled[:, i * unit : (i + 1) * unit] * gain_ref[i : i + 1, :].astype(F32)
+            ).astype(BF16)
+            for i in range(width // unit)
+        ],
+        axis=1,
+    )
     routed = dot(placing, normed).astype(BF16)
     total[...] = residual
 
@@ -277,9 +293,6 @@
         for s in range(segs):
             stack[pl.ds(s * crows, crows)] = value[:, s * SEG : (s + 1) * SEG]
         target[...] = dot(spread[...], stack[...]).astype(BF16)
-
-    for c in range(chunks):
-        to_blocks(routed[c * crows : (c + 1) * crows], go.at[c])
 
     def send_blocks(source, target, c, send, recv):
         own = pl.ds(pl.multiple_of(me * block, block), block)
@@ -344,8 +357,10 @@
         )
 
     ahead = min(AHEAD, chunks)
-    for c in range(ahead):
-        send_blocks(go, came, c, go_send, go_recv)
+    for c in range(chunks):
+        to_blocks(routed[c * crows : (c + 1) * crows], go.at[c])
+        if c < ahead:
+            send_blocks(go, came, c, go_send, go_recv)
     for copy in weight_copies():
         copy.wait()
 
@@ -508,6 +523,7 @@
         vmem((chunks, size, SEG), BF16),
         vmem((chunks, size, SEG), BF16),
         vmem((tokens, width), F32),
+        pltpu.SemaphoreType.REGULAR((max(1, n.bit_length()),)),
         dma((2 * tiles + cols,)),
         dma((2,)),
         dma((lanes - 1,)),
@@ -541,7 +557,7 @@
         group_map,
         pool_scale.reshape(1, -1),
         out_proj,
-        norm_gain.reshape(1, -1),
+        norm_gain.reshape(-1, 128),
         routes.T,
         route_weight.T,
         expert_gate,

time: 185 us -> 179 us (0.968)
  Pallas kernels: 181 us -> 177 us
    pallas_call x1, Pallas kernels: 181 us -> 177 us  [local(): pl.pallas_call(functools.partial(kernel, (n, lanes, chunks, slots)), out_...]
where the time goes in v3:
time: 179 us
  Pallas kernels  177 us (99%)
  local copies, waits for them, and re-layouts  1.88 us (1%)
    pallas_call x1, Pallas kernels, local(): pl.pallas_call(functools.partial(kernel, (n, lanes, chunks, slots)), out_...  177 us

profile of v3, /device:TPU:33, one launch (start us, length us, event | category | flops | bytes accessed | tf_op | source)
XLA Modules:
  0.0 178.6 jit_solution(16745734155294814397)
XLA Ops:
  0.0 176.7 %layer.1 = bf16[128,2048]{1,0:T(8,128)(2,1)} custom-call(bf16[128,2048]{1,0:T(8,128)(2,1)} %resid_ref.1, bf16[512,128]{1,0:T(8,128)(2,1)} %pool_ref.1, bf16[1,128,128]{2,1,0:T(8,128)(2,1)} %map_ref.1, bf16[1,128]{1,0:T(2,128)(2,1)} %bitcast.7, bf16[128,2048]{1,0:T(8,128)(2,1)} %proj_ref.1, bf16[16,128]{1,0:T(8,128)(2,1)} %bitcast.4, s32[2,128]{1,0:T(2,128)} %bitcast.5, ...), custom_call_target="tpu_custom_call" | custom-call | tf_op jit(solution)/shard_map/layer/pallas_call | solution.py:544
  176.8 1.9 %copy.13 = bf16[128,2048]{1,0:T(8,128)(2,1)} copy(bf16[128,2048]{1,0:T(8,128)(2,1)} %layer.1) | data formatting | bytes 1048576

commit v4 on v3

--- a/solution.py
+++ b/solution.py
@@ -23,9 +23,9 @@
     ("send_next", -AHEAD),
     ("experts", 1),
     ("relay", 0),
+    ("give_back", 2),
     ("add_far", 1),
-    ("give_back", 2),
-    ("combine", 3),
+    ("combine", 4),
 )
 
 
@@ -37,13 +37,32 @@
     return jnp.dot(a, b, preferred_element_type=F32)
 
 
+def quot(a, b):
+    return jnp.right_shift(a, b.bit_length() - 1) if b & (b - 1) == 0 else a // b
+
+
+def rem(a, b):
+    return jnp.bitwise_and(a, b - 1) if b & (b - 1) == 0 else lax.rem(a, b)
+
+
 def settle(like, sem):
     pltpu.make_async_copy(like, like, sem).wait()
 
 
 def kernel(
     sizes,
-    resid_ref,
+    resid_hbm,
+    pool_hbm,
+    map_hbm,
+    scale_hbm,
+    proj_hbm,
+    gain_hbm,
+    routes_hbm,
+    weight_hbm,
+    gate_hbm,
+    up_hbm,
+    down_hbm,
+    out_ref,
     pool_ref,
     map_ref,
     scale_ref,
@@ -51,10 +70,6 @@
     gain_ref,
     routes_ref,
     weight_ref,
-    gate_hbm,
-    up_hbm,
-    down_hbm,
-    out_ref,
     ext,
     halo,
     pieces,
@@ -79,6 +94,8 @@
     home,
     total,
     known,
+    resid_sem,
+    in_sem,
     w_sem,
     halo_sem,
     proj_send,
@@ -97,8 +114,8 @@
     back_recv,
 ):
     n, lanes, chunks, slots = sizes
-    tokens, width = resid_ref.shape
-    seq_rows, gdim = pool_ref.shape
+    tokens, width = resid_hbm.shape
+    seq_rows, gdim = pool_hbm.shape
     segs = width // SEG
     block = PAIR * segs
     crows = PAIR * n
@@ -138,32 +155,24 @@
             barrier, inc=1, device_id={"tp": tp_at(k)}, device_id_type=MESH
         )
 
-    size = n * block
-    a, b = iota((size, size), 0), iota((size, size), 1)
-    seg_a, rest = a // crows, lax.rem(a, crows)
-    where = (rest // PAIR) * block + seg_a * PAIR + lax.rem(rest, PAIR)
-    gather[...] = (b == where).astype(F32).astype(BF16)
-    seg_b, rest_b = b // crows, lax.rem(b, crows)
-    where_b = (rest_b // PAIR) * block + seg_b * PAIR + lax.rem(rest_b, PAIR)
-    spread[...] = (a == where_b).astype(F32).astype(BF16)
-
-    one0 = (iota((n, tokens), 0) == routes_ref[0:1, :]).astype(F32)
-    one1 = (iota((n, tokens), 0) == routes_ref[1:2, :]).astype(F32)
-    before = (iota((tokens, tokens), 0) < iota((tokens, tokens), 1)).astype(F32).astype(BF16)
-    rank0 = dot(one0.astype(BF16), before)
-    rank1 = dot(one1.astype(BF16), before) + jnp.sum(one0, axis=1, keepdims=True)
-    slot0 = jnp.sum(rank0 * one0, axis=0, keepdims=True).astype(I32)
-    slot1 = jnp.sum(rank1 * one1, axis=0, keepdims=True).astype(I32)
-    row0 = (slot0 // PAIR) * crows + routes_ref[0:1, :] * PAIR + lax.rem(slot0, PAIR)
-    row1 = (slot1 // PAIR) * crows + routes_ref[1:2, :] * PAIR + lax.rem(slot1, PAIR)
-    place = iota((chunks * crows, tokens), 0)
-    hit0, hit1 = place == row0, place == row1
-    weight = jnp.where(hit0, weight_ref[0:1, :], 0.0) + jnp.where(hit1, weight_ref[1:2, :], 0.0)
-    high = weight.astype(BF16)
-    w_hi[...] = high.reshape(chunks, crows, tokens)
-    w_lo[...] = (weight - high.astype(F32)).astype(BF16).reshape(chunks, crows, tokens)
-    placing = (jnp.where(hit0, 1.0, 0.0) + jnp.where(hit1, 1.0, 0.0)).astype(BF16)
-
+    small = {
+        name: pltpu.make_async_copy(source, target, in_sem.at[i])
+        for i, (name, source, target) in enumerate(
+            (
+                ("proj", proj_hbm, proj_ref),
+                ("pool", pool_hbm, pool_ref),
+                ("map", map_hbm, map_ref),
+                ("scale", scale_hbm, scale_ref),
+                ("gain", gain_hbm, gain_ref),
+                ("routes", routes_hbm, routes_ref),
+                ("weight", weight_hbm, weight_ref),
+            )
+        )
+    }
+    for copy in small.values():
+        copy.start()
+    small["pool"].wait()
+    small["proj"].wait()
     pl.semaphore_wait(barrier, 2 + lanes - 1)
 
     halo_copy = remote(
@@ -199,11 +208,54 @@
     for k in order:
         proj_copy(k).start()
 
+    size = n * block
+
+    def block_row(a):
+        rest = rem(a, crows)
+        return quot(rest, PAIR) * block + quot(a, crows) * PAIR + rem(rest, PAIR)
+
+    def fill_gather():
+        gather[...] = jnp.where(
+            iota((size, size), 1) == block_row(iota((size, 1), 0)), 1.0, 0.0
+        ).astype(BF16)
+
+    def fill_spread():
+        spread[...] = jnp.where(
+            iota((size, size), 0) == block_row(iota((1, size), 1)), 1.0, 0.0
+        ).astype(BF16)
+
+    resid_copy = pltpu.make_async_copy(resid_hbm, mixed, resid_sem)
+    resid_copy.start()
+
     radius, level = 1, 0
+    work = [fill_gather, fill_spread]
     while radius < n // 2:
         greet(known.at[level], radius)
+        if work:
+            work.pop(0)()
         pl.semaphore_wait(known.at[level], 2)
         radius, level = 2 * radius, level + 1
+    for left_over in work:
+        left_over()
+
+    for name in ("map", "scale", "gain", "routes", "weight"):
+        small[name].wait()
+    one0 = (iota((n, tokens), 0) == routes_ref[0:1, :]).astype(F32)
+    one1 = (iota((n, tokens), 0) == routes_ref[1:2, :]).astype(F32)
+    before = (iota((tokens, tokens), 0) < iota((tokens, tokens), 1)).astype(F32).astype(BF16)
+    rank0 = dot(one0.astype(BF16), before)
+    rank1 = dot(one1.astype(BF16), before) + jnp.sum(one0, axis=1, keepdims=True)
+    slot0 = jnp.sum(rank0 * one0, axis=0, keepdims=True).astype(I32)
+    slot1 = jnp.sum(rank1 * one1, axis=0, keepdims=True).astype(I32)
+    row0 = quot(slot0, PAIR) * crows + routes_ref[0:1, :] * PAIR + rem(slot0, PAIR)
+    row1 = quot(slot1, PAIR) * crows + routes_ref[1:2, :] * PAIR + rem(slot1, PAIR)
+    place = iota((chunks * crows, tokens), 0)
+    hit0, hit1 = place == row0, place == row1
+    weight = jnp.where(hit0, weight_ref[0:1, :], 0.0) + jnp.where(hit1, weight_ref[1:2, :], 0.0)
+    high = weight.astype(BF16)
+    w_hi[...] = high.reshape(chunks, crows, tokens)
+    w_lo[...] = (weight - high.astype(F32)).astype(BF16).reshape(chunks, crows, tokens)
+    placing = (jnp.where(hit0, 1.0, 0.0) + jnp.where(hit1, 1.0, 0.0)).astype(BF16)
 
     tiles = w_gu.shape[0]
     cols = w_down.shape[0]
@@ -270,8 +322,8 @@
         piece_copy(k).wait_recv()
         settle(proj_in.at[k - 1, other], mate_recv.at[k - 1])
         mix = mix + dot(piece_in[k - 1], proj_in[k - 1])
-    mixed_value = (resid_ref[...].astype(F32) + mix).astype(BF16)
-    mixed[...] = mixed_value
+    resid_copy.wait()
+    mixed_value = (mixed[...].astype(F32) + mix).astype(BF16)
     residual = mixed_value.astype(F32)
     scaled = residual * lax.rsqrt(
         jnp.sum(residual * residual, axis=1, keepdims=True) / width + norm_eps
@@ -309,12 +361,12 @@
             return carry
 
         def both(k, carry):
-            one(k, 0)
-            one(n - k, 0)
+            one(n // 2 - k, 0)
+            one(n // 2 + k, 0)
             return carry
 
+        one(n // 2, 0)
         lax.fori_loop(1, n // 2, both, 0)
-        one(n // 2, 0)
 
     def take_blocks(source, target, c, recv):
         own = pl.ds(pl.multiple_of(me * block, block), block)
@@ -500,6 +552,13 @@
     vmem, dma = pltpu.VMEM, pltpu.SemaphoreType.DMA
     hbm = pl.BlockSpec(memory_space=pl.ANY)
     scratch = [
+        vmem(pool_input.shape, BF16),
+        vmem(group_map.shape, BF16),
+        vmem((1, gdim), BF16),
+        vmem(out_proj.shape, BF16),
+        vmem((width // 128, 128), BF16),
+        vmem(routes.shape[::-1], I32),
+        vmem(route_weight.shape[::-1], F32),
         vmem((HALO + seq_rows, gdim), F32),
         vmem((HALO, gdim), BF16),
         vmem((seq_rows, gdim), BF16),
@@ -524,6 +583,8 @@
         vmem((chunks, size, SEG), BF16),
         vmem((tokens, width), F32),
         pltpu.SemaphoreType.REGULAR((max(1, n.bit_length()),)),
+        dma,
+        dma((7,)),
         dma((2 * tiles + cols,)),
         dma((2,)),
         dma((lanes - 1,)),
@@ -544,7 +605,7 @@
     return pl.pallas_call(
         functools.partial(kernel, (n, lanes, chunks, slots)),
         out_shape=jax.ShapeDtypeStruct((tokens, width), BF16),
-        in_specs=[pl.BlockSpec(memory_space=vmem)] * 8 + [hbm] * 3,
+        in_specs=[hbm] * 11,
         out_specs=pl.BlockSpec(memory_space=vmem),
         scratch_shapes=scratch,
         compiler_params=pltpu.CompilerParams(

time: 179 us -> 170 us (0.950)
  Pallas kernels: 177 us -> 168 us
    pallas_call x1, Pallas kernels: 177 us -> 168 us  [local(): pl.pallas_call(functools.partial(kernel, (n, lanes, chunks, slots)), out_...]
where the time goes in v4:
time: 170 us
  Pallas kernels  168 us (99%)
  local copies, waits for them, and re-layouts  1.88 us (1%)
    pallas_call x1, Pallas kernels, local(): pl.pallas_call(functools.partial(kernel, (n, lanes, chunks, slots)), out_...  168 us

profile of v4, /device:TPU:33, one launch (start us, length us, event | category | flops | bytes accessed | tf_op | source)
XLA Modules:
  0.0 169.7 jit_solution(14313804951359600645)
XLA Ops:
  0.0 167.8 %layer.1 = bf16[128,2048]{1,0:T(8,128)(2,1)} custom-call(bf16[128,2048]{1,0:T(8,128)(2,1)} %resid_hbm.1, bf16[512,128]{1,0:T(8,128)(2,1)} %pool_hbm.1, bf16[1,128,128]{2,1,0:T(8,128)(2,1)} %map_hbm.1, bf16[1,128]{1,0:T(2,128)(2,1)} %bitcast.7, bf16[128,2048]{1,0:T(8,128)(2,1)} %proj_hbm.1, bf16[16,128]{1,0:T(8,128)(2,1)} %bitcast.4, s32[2,128]{1,0:T(2,128)} %bitcast.5, ...), custom_call_target="tpu_custom_call" | custom-call | tf_op jit(solution)/shard_map/layer/pallas_call | solution.py:605
  167.8 1.9 %copy.13 = bf16[128,2048]{1,0:T(8,128)(2,1)} copy(bf16[128,2048]{1,0:T(8,128)(2,1)} %layer.1) | data formatting | bytes 1048576
